TPU v7x, 32 devices: a whole 2x2x4 slice. The times are simulated.
32 devices in a mesh: grp: 2 (over x), ep: 16 (over z, y, core).
Axes of the slice: x: 2, y: 2, z: 4, core: 2. Of those that a mesh axis runs over, the one named last changes fastest.
Arguments:
- hidden: bfloat16 [96, 2048], P(('grp', 'ep')), parts along dimension 0, may hold values from -6 to 6
- conv_window: bfloat16 [96, 3, 6144], P(('grp', 'ep')), parts along dimension 0, may hold values from -6 to 6
- ssm_state: float32 [96, 64, 64, 128], P(('grp', 'ep')), parts along dimension 0, may hold values from -1.75 to 1.75
- gate_proj: bfloat16 [2048, 4096], P(None, 'ep'), may hold values from -0.125 to 0.125
- input_proj: bfloat16 [2048, 4096], P(None, 'ep'), may hold values from -0.125 to 0.125
- write_proj: bfloat16 [2048, 1024], P(None, 'ep'), may hold values from -0.125 to 0.125
- read_proj: bfloat16 [2048, 1024], P(None, 'ep'), may hold values from -0.125 to 0.125
- step_proj: bfloat16 [2048, 64], replicated, may hold values from -0.125 to 0.125
- step_bias: float32 [64], replicated, may hold values from -2 to 1
- decay_log: float32 [64], replicated, may hold values from -2.3 to 1.4
- decay_shift: float32 [96, 64], P(('grp', 'ep')), parts along dimension 0, may hold values from -0.7 to 0
- skip_scale: float32 [64], replicated, may hold values from -4 to 4
- conv_taps: bfloat16 [4, 6144], replicated, may hold values from -3 to 3
- conv_bias: float32 [6144], replicated, may hold values from -3 to 3
- mix_gain: float32 [2048], replicated, may hold values from 0.1 to 1.9
- group_gain: float32 [4096], replicated, may hold values from 0.1 to 1.9
- out_proj: bfloat16 [4096, 2048], P(None, 'ep'), may hold values from -0.09375 to 0.09375
- ffn_gain: float32 [2048], replicated, may hold values from 0.1 to 1.9
- router: bfloat16 [2048, 16], replicated, may hold values from -0.125 to 0.125
- expert_ids: int32 [96, 6], P(('grp', 'ep')), parts along dimension 0, may hold values from 0 to 15, all different within a row; in each aligned block of 3 rows (0 to 2, 3 to 5, ...) at most 2 rows name the same one
- expert_gate: bfloat16 [16, 2048, 512], P('ep'), may hold values from -0.125 to 0.125
- expert_up: bfloat16 [16, 2048, 512], P('ep'), may hold values from -0.125 to 0.125
- expert_down: bfloat16 [16, 512, 2048], P('ep'), may hold values from -0.25 to 0.25
- shared_gate: bfloat16 [2048, 512], P('ep'), may hold values from -0.125 to 0.125
- shared_up: bfloat16 [2048, 512], P('ep'), may hold values from -0.125 to 0.125
- shared_down: bfloat16 [512, 2048], replicated, may hold values from -0.25 to 0.25
Outputs:
- layer_out: bfloat16 [96, 2048], P(('grp', 'ep')), parts along dimension 0
- next_state: float32 [96, 64, 64, 128], P(('grp', 'ep')), parts along dimension 0
- next_window: bfloat16 [96, 3, 6144], P(('grp', 'ep')), parts along dimension 0
There are 2 independent parts, one for each index of `grp`. A program takes and returns all parts, laid end to end along the dimension named above; an argument that names none is the same for every part. Nothing has to cross between parts.
Inputs may be any that keep to these rules, and one draw needn't show every extreme that they name: `expert_ids`: each row names 6 different experts; in the rows of one device no expert is named by more than 2 rows, and in every draw some device's rows name some expert exactly 2 times.
All inputs are finite; a program needn't handle non-finite values.
Results may differ from a plain program's by a relative error of at most 0.019.
Values may be sent and summed in bfloat16 or wider, within the bound.
A program may use at most 128 MiB of HBM per device.

v0:
```python
import jax
import jax.numpy as jnp
from jax import lax
from jax.sharding import PartitionSpec as P

HEAD_DIM = 64
GROUPS = 8
STATE = 128
CAP = 2
epsilon = 1e-06
routed_scale = 2.5


def row_scale(values):
    return lax.rsqrt(jnp.mean(values * values, axis=-1, keepdims=True) + epsilon)


def matmul(left, right):
    return jnp.dot(left, right, preferred_element_type=jnp.float32)


def expert_result(rows_in, weight_gate, weight_up, weight_down):
    expert_hidden = (jax.nn.silu(matmul(rows_in, weight_gate)) * matmul(rows_in, weight_up)).astype(
        jnp.bfloat16
    )
    return matmul(expert_hidden, weight_down).astype(jnp.bfloat16)


def route_weights(routed_in, router, chosen):
    scores = jax.nn.sigmoid(matmul(routed_in, router))
    picked = jnp.take_along_axis(scores, chosen, axis=1)
    return routed_scale * picked / jnp.sum(picked, axis=1, keepdims=True)


def shards(
    hidden,
    conv_window,
    ssm_state,
    gate_proj,
    input_proj,
    write_proj,
    read_proj,
    step_proj,
    step_bias,
    decay_log,
    decay_shift,
    skip_scale,
    conv_taps,
    conv_bias,
    mix_gain,
    group_gain,
    out_proj,
    ffn_gain,
    router,
    expert_ids,
    expert_gate,
    expert_up,
    expert_down,
    shared_gate,
    shared_up,
    shared_down,
):
    local_rows = hidden.shape[0]
    device_index = lax.axis_index("ep")
    gathered = lax.all_gather(hidden, "ep", axis=0, tiled=True)
    gathered_wide = gathered.astype(jnp.float32)
    normed = (gathered_wide * row_scale(gathered_wide) * mix_gain).astype(jnp.bfloat16)
    gate_part = matmul(normed, gate_proj).astype(jnp.bfloat16)
    input_part = matmul(normed, input_proj).astype(jnp.bfloat16)
    write_part = matmul(normed, write_proj).astype(jnp.bfloat16)
    read_part = matmul(normed, read_proj).astype(jnp.bfloat16)
    gate_rows, input_rows, write_rows, read_rows = (
        lax.all_to_all(gate_part, "ep", split_axis=0, concat_axis=1, tiled=True),
        lax.all_to_all(input_part, "ep", split_axis=0, concat_axis=1, tiled=True),
        lax.all_to_all(write_part, "ep", split_axis=0, concat_axis=1, tiled=True),
        lax.all_to_all(read_part, "ep", split_axis=0, concat_axis=1, tiled=True),
    )
    normed_local = lax.dynamic_slice_in_dim(normed, device_index * local_rows, local_rows, 0)
    step_raw = matmul(normed_local, step_proj)
    inner_width = gate_rows.shape[1]
    state_span = GROUPS * STATE
    head_count = step_bias.shape[0]
    per_group = head_count // GROUPS
    fresh_row = jnp.concatenate([input_rows, write_rows, read_rows], axis=1)
    window = jnp.concatenate([conv_window, fresh_row[:, None, :]], axis=1)
    convolved = jax.nn.silu(
        jnp.sum(window.astype(jnp.float32) * conv_taps.astype(jnp.float32)[None], axis=1)
        + conv_bias
    )
    head_input = convolved[:, :inner_width].reshape(local_rows, GROUPS, per_group, HEAD_DIM)
    write_vec = convolved[:, inner_width : inner_width + state_span].reshape(
        local_rows, GROUPS, STATE
    )
    read_vec = convolved[:, inner_width + state_span :].reshape(local_rows, GROUPS, STATE)
    step_size = jax.nn.softplus(step_raw + step_bias)
    decay_rate = jnp.exp(decay_shift - step_size * jnp.exp(decay_log)).reshape(
        local_rows, GROUPS, per_group
    )
    step_group = step_size.reshape(local_rows, GROUPS, per_group)
    carried = ssm_state.reshape(local_rows, GROUPS, per_group, HEAD_DIM, STATE)
    next_state = (
        decay_rate[..., None, None] * carried
        + (step_group[..., None] * head_input)[..., None] * write_vec[:, :, None, None, :]
    )
    mixed_out = jnp.einsum("sgepn,sgn->sgep", next_state, read_vec, precision=lax.Precision.HIGHEST)
    mixed_out = mixed_out + skip_scale.reshape(GROUPS, per_group)[None, :, :, None] * head_input
    mixed_out = mixed_out.reshape(local_rows, inner_width).astype(jnp.bfloat16)
    gated_out = mixed_out.astype(jnp.float32) * jax.nn.silu(gate_rows.astype(jnp.float32))
    blocks = gated_out.reshape(local_rows, GROUPS, -1)
    gated_out = ((blocks * row_scale(blocks)).reshape(local_rows, inner_width) * group_gain).astype(
        jnp.bfloat16
    )
    col_width = out_proj.shape[1]
    resid_cols = lax.dynamic_slice_in_dim(gathered_wide, device_index * col_width, col_width, 1)
    resid_part = (
        resid_cols + matmul(lax.all_gather(gated_out, "ep", axis=0, tiled=True), out_proj)
    ).astype(jnp.bfloat16)
    gain_part = lax.dynamic_slice_in_dim(ffn_gain, device_index * col_width, col_width, 0)
    shared_part = (resid_part.astype(jnp.float32) * gain_part).astype(jnp.bfloat16)
    shared_pre = lax.psum_scatter(
        jnp.concatenate(
            [matmul(shared_part, shared_gate), matmul(shared_part, shared_up)], axis=1
        ).astype(jnp.bfloat16),
        "ep",
        scatter_dimension=0,
        tiled=True,
    ).astype(jnp.float32)
    exp_dev = expert_gate.shape[0]
    resid = lax.all_to_all(resid_part, "ep", split_axis=0, concat_axis=1, tiled=True)
    resid_wide = resid.astype(jnp.float32)
    norm_scale = row_scale(resid_wide)
    routed_in = (resid_wide * norm_scale * ffn_gain).astype(jnp.bfloat16)
    weights = route_weights(routed_in, router, expert_ids)
    expert_total = router.shape[1]
    member = jnp.any(
        expert_ids[:, :, None] == jnp.arange(expert_total, dtype=jnp.int32)[None, None, :], axis=1
    ).astype(jnp.int32)
    earlier = jnp.cumsum(member, axis=0) - member
    slot_index = jnp.take_along_axis(earlier, expert_ids, axis=1)
    places = expert_ids * CAP + slot_index
    dispatch_table = jnp.any(
        places[None, :, :] == jnp.arange(expert_total * CAP, dtype=jnp.int32)[:, None, None], axis=2
    ).astype(jnp.bfloat16)
    outbound = (
        matmul(dispatch_table, routed_in)
        .astype(jnp.bfloat16)
        .reshape(lax.axis_size("ep"), exp_dev, CAP, routed_in.shape[1])
    )
    arrived = lax.all_to_all(outbound, "ep", split_axis=0, concat_axis=0, tiled=True)
    rows_in = arrived[:, 0].reshape(-1, arrived.shape[-1])
    result = expert_result(rows_in, expert_gate[0], expert_up[0], expert_down[0])
    results = [result.reshape(arrived.shape[0], arrived.shape[2], arrived.shape[3])]
    returned = lax.all_to_all(
        jnp.stack(results, axis=1), "ep", split_axis=0, concat_axis=0, tiled=True
    )
    returned_flat = returned.reshape(expert_total * CAP, returned.shape[-1])
    picked = jnp.take(returned_flat, places.reshape(-1), axis=0).reshape(
        local_rows, expert_ids.shape[1], returned.shape[-1]
    )
    routed = jnp.sum(picked.astype(jnp.float32) * weights[:, :, None], axis=1)
    hidden_units = shared_down.shape[0]
    shared_hidden = (
        jax.nn.silu(norm_scale * shared_pre[:, :hidden_units])
        * (norm_scale * shared_pre[:, hidden_units:])
    ).astype(jnp.bfloat16)
    layer_out = (resid_wide + routed + matmul(shared_hidden, shared_down)).astype(jnp.bfloat16)
    return (layer_out, next_state.reshape(ssm_state.shape), window[:, 1:])


def solution(mesh):
    placed = (
        P(("grp", "ep"), None),
        P(("grp", "ep"), None, None),
        P(("grp", "ep"), None, None, None),
        P(None, "ep"),
        P(None, "ep"),
        P(None, "ep"),
        P(None, "ep"),
        P(),
        P(),
        P(),
        P(("grp", "ep"), None),
        P(),
        P(),
        P(),
        P(),
        P(),
        P(None, "ep"),
        P(),
        P(),
        P(("grp", "ep"), None),
        P("ep", None, None),
        P("ep", None, None),
        P("ep", None, None),
        P("ep", None),
        P("ep", None),
        P(),
    )
    return jax.shard_map(
        shards,
        mesh=mesh,
        in_specs=placed,
        out_specs=(
            P(("grp", "ep"), None),
            P(("grp", "ep"), None, None, None),
            P(("grp", "ep"), None, None),
        ),
        check_vma=False,
    )
```

profile of v0, /device:TPU:0, one launch (start us, length us, event | category | flops | bytes accessed | tf_op | source)
XLA Modules:
  0.0 219.6 jit_solution(2211372966477305906)
XLA Ops:
  7.3 24.2 %all-gather = bf16[16,3,2048]{2,1,0:T(4,128)(2,1)S(1)} all-gather(bf16[1,3,2048]{2,1,0:T(4,128)(2,1)} %bitcast.106), channel_id=1, replica_groups=mesh['grp'=2,'ep'=16] {'ep'}, dimensions={0}, use_global_device_ids=true | all-gather | bytes 208896 | tf_op jit(solution)/shard_map/all_gather | solution.py:65
  31.8 0.8 multiply_convert_fusion
  32.6 1.2 convolution_convert_fusion.7
  34.4 3.5 %all-to-all-start.1 = ((bf16[16,3,64]{2,1,0:T(4,128)(2,1)}), bf16[16,3,64]{2,1,0:T(4,128)(2,1)S(1)}, u32[]{:S(2)}, u32[]{:S(2)}) async-start(bf16[16,3,64]{2,1,0:T(4,128)(2,1)} %all_to_all.72), calls=%async_computation.1 | async-start | bytes 32768 | tf_op jit(solution)/shard_map/all_to_all | solution.py:75
  37.9 0.8 fusion.42
  39.4 1.5 convolution_convert_fusion.5
  40.9 1.2 convolution_convert_fusion.6
  42.7 1.5 convolution_convert_fusion.4
  44.4 0.8 gather_fusion.1
  46.3 6.0 %all-to-all-start.2 = ((bf16[16,3,64]{2,1,0:T(4,128)(2,1)}), bf16[16,3,64]{2,1,0:T(4,128)(2,1)S(1)}, u32[]{:S(2)}, u32[]{:S(2)}) async-start(bf16[16,3,64]{2,1,0:T(4,128)(2,1)} %all_to_all.76), calls=%async_computation.2 | async-start | bytes 32768 | tf_op jit(solution)/shard_map/all_to_all | solution.py:76
  53.0 5.8 %all-to-all-done.2 = bf16[16,3,64]{2,1,0:T(4,128)(2,1)S(1)} async-done(((bf16[16,3,64]{2,1,0:T(4,128)(2,1)}), bf16[16,3,64]{2,1,0:T(4,128)(2,1)S(1)}, u32[]{:S(2)}, u32[]{:S(2)}) %all-to-all-start.2) | async-done | bytes 6176 | tf_op jit(solution)/shard_map/all_to_all | solution.py:76
  58.7 3.5 %all-to-all-start = ((bf16[16,3,256]{2,1,0:T(4,128)(2,1)}), bf16[16,3,256]{2,1,0:T(4,128)(2,1)S(1)}, u32[]{:S(2)}, u32[]{:S(2)}) async-start(bf16[16,3,256]{2,1,0:T(4,128)(2,1)} %all_to_all.68), calls=%async_computation | async-start | bytes 65536 | tf_op jit(solution)/shard_map/all_to_all | solution.py:74
  64.7 4.2 %all-to-all-done = bf16[16,3,256]{2,1,0:T(4,128)(2,1)S(1)} async-done(((bf16[16,3,256]{2,1,0:T(4,128)(2,1)}), bf16[16,3,256]{2,1,0:T(4,128)(2,1)S(1)}, u32[]{:S(2)}, u32[]{:S(2)}) %all-to-all-start) | async-done | bytes 24608 | tf_op jit(solution)/shard_map/all_to_all | solution.py:74
  68.9 3.5 %all-to-all-start.3 = ((bf16[16,3,256]{2,1,0:T(4,128)(2,1)}), bf16[16,3,256]{2,1,0:T(4,128)(2,1)S(1)}, u32[]{:S(2)}, u32[]{:S(2)}) async-start(bf16[16,3,256]{2,1,0:T(4,128)(2,1)} %all_to_all.80), calls=%async_computation.3 | async-start | bytes 65536 | tf_op jit(solution)/shard_map/all_to_all | solution.py:73
  72.5 0.9 fusion.25
  74.7 4.2 %all-to-all-done.3 = bf16[16,3,256]{2,1,0:T(4,128)(2,1)S(1)} async-done(((bf16[16,3,256]{2,1,0:T(4,128)(2,1)}), bf16[16,3,256]{2,1,0:T(4,128)(2,1)S(1)}, u32[]{:S(2)}, u32[]{:S(2)}) %all-to-all-start.3) | async-done | bytes 24608 | tf_op jit(solution)/shard_map/all_to_all | solution.py:73
  79.2 16.8 %fusion = f32[3,8,1,8,64]{4,2,3,1,0:T(1,128)S(1)} fusion(f32[3,8,128,1,1]{2,3,4,1,0:T(1,128)S(1)} %bitcast.105, f32[3,8,8,64,128]{4,3,2,1,0:T(8,128)} %bitcast.96, f32[3,8,128]{2,1,0:T(8,128)S(1)} %bitcast.102, f32[3,8,8,64]{3,2,1,0:T(8,128)S(1)} %broadcast_multiply_fusion.1, f32[3,8,8]{2,1,0:T(8,128)S(1)} %mul.238), kind=kOutput, calls=%fused_computation.4 | convolution fusion | flops 23592960 | bytes 6415104 | tf_op jit(solution)/shard_map/sgepn,sgn->sgep/dot_general | solution.py:105
  96.5 19.0 %all-gather.1 = bf16[16,3,4096]{2,1,0:T(4,128)(2,1)S(1)} all-gather(bf16[1,3,4096]{2,1,0:T(4,128)(2,1)S(1)} %fusion.40), channel_id=1, replica_groups=mesh['grp'=2,'ep'=16] {'ep'}, dimensions={0}, use_global_device_ids=true | all-gather | bytes 417792 | tf_op jit(solution)/shard_map/all_gather | solution.py:116
  115.9 1.5 fusion.21
  118.0 1.0 convolution_convert_fusion.2
  119.1 1.0 convolution_convert_fusion.3
  120.8 3.5 %all-to-all-start.4 = ((bf16[16,3,128]{2,1,0:T(4,128)(2,1)}), bf16[16,3,128]{2,1,0:T(4,128)(2,1)S(1)}, u32[]{:S(2)}, u32[]{:S(2)}) async-start(bf16[16,3,128]{2,1,0:T(4,128)(2,1)} %all_to_all.82), calls=%async_computation.4 | async-start | bytes 32768 | tf_op jit(solution)/shard_map/all_to_all | solution.py:129
  124.3 1.0 broadcast_multiply_fusion
  125.3 7.0 %multiply_add_fusion = f32[3,64,64,128]{3,2,1,0:T(8,128)} fusion(f32[3,64,64,128]{3,2,1,0:T(8,128)} %param.28, f32[3,64,128]{2,1,0:T(8,128)S(1)} %broadcast_bitcast_fusion, f32[3,64,64]{2,1,0:T(8,128)S(1)} %broadcast_multiply_fusion, f32[3,64]{1,0:T(4,128)S(1)} %get-tuple-element.11), kind=kLoop, calls=%fused_computation.3 | loop fusion | flops 4718592 | bytes 12731136 | tf_op jit(solution)/shard_map/add | solution.py:102
  133.4 6.0 %all-to-all-start.5 = ((bf16[16,1,2,2048]{3,2,1,0:T(2,128)(2,1)}), bf16[16,1,2,2048]{3,2,1,0:T(2,128)(2,1)S(1)}, u32[]{:S(2)}, u32[]{:S(2)}) async-start(bf16[16,1,2,2048]{3,2,1,0:T(2,128)(2,1)} %bitcast.18), calls=%async_computation.5 | async-start | bytes 262144 | tf_op jit(solution)/shard_map/all_to_all | solution.py:149
  139.6 0.9 gather_fusion.2
  140.7 6.7 %all-to-all-done.5 = bf16[16,1,2,2048]{3,2,1,0:T(2,128)(2,1)S(1)} async-done(((bf16[16,1,2,2048]{3,2,1,0:T(2,128)(2,1)}), bf16[16,1,2,2048]{3,2,1,0:T(2,128)(2,1)S(1)}, u32[]{:S(2)}, u32[]{:S(2)}) %all-to-all-start.5) | async-done | bytes 131104 | tf_op jit(solution)/shard_map/all_to_all | solution.py:149
  147.4 2.0 fusion.11
  149.4 2.5 %convolution_convert_fusion = bf16[32,2048]{1,0:T(8,128)(2,1)S(1)} fusion(bf16[1,512,2048]{2,1,0:T(8,128)(2,1)S(1)} %copy-done, bf16[32,2048]{1,0:T(8,128)(2,1)S(1)} %reshape_squeeze.3, bf16[1,2048,512]{2,1,0:T(8,128)(2,1)} %param.47, f32[32,512]{1,0:T(8,128)S(1)} %fusion.11), kind=kOutput, calls=%fused_computation.11 | convolution fusion | flops 134381568 | bytes 4521984 | tf_op jit(solution)/shard_map/dot_general | solution.py:19
  152.7 3.5 %all-to-all-start.6 = ((bf16[16,1,2,2048]{3,2,1,0:T(2,128)(2,1)}), bf16[16,1,2,2048]{3,2,1,0:T(2,128)(2,1)S(1)}, u32[]{:S(2)}, u32[]{:S(2)}) async-start(bf16[16,1,2,2048]{3,2,1,0:T(2,128)(2,1)} %bitcast.22), calls=%async_computation.6 | async-start | bytes 262144 | tf_op jit(solution)/shard_map/all_to_all | solution.py:153
  156.3 52.1 %all-reduce.3.cloned.1.call-done = bf16[48,1024]{1,0:T(8,128)(2,1)} async-done(((bf16[48,1024]{1,0:T(8,128)(2,1)}), bf16[48,1024]{1,0:T(8,128)(2,1)}) %all-reduce.3.cloned.1.call-update) | async-done | bytes 98320
  210.1 2.6 %fusion.7 = bf16[3,2048]{1,0:T(4,128)(2,1)} fusion(bf16[512,2048]{1,0:T(8,128)(2,1)} %param.51, f32[3,2048]{1,0:T(4,128)S(1)} %multiply_reduce_fusion.2, bf16[16,3,128]{2,1,0:T(4,128)(2,1)S(1)} %all-to-all-done.4, f32[3,1024]{1,0:T(4,128)S(1)} %dynamic-slice_convert_fusion, f32[3]{0:T(128)S(1)} %add_rsqrt_fusion.1), kind=kOutput, calls=%fused_computation.14 | convolution fusion | flops 6328320 | bytes 2158604 | tf_op jit(solution)/shard_map/dot_general | solution.py:19
  (100 shorter events, 13.7 us)
Async XLA Ops:
  7.2 142.3 %copy-start = (bf16[1,512,2048]{2,1,0:T(8,128)(2,1)S(1)}, bf16[1,512,2048]{2,1,0:T(8,128)(2,1)}, u32[]{:S(2)}) copy-start(bf16[1,512,2048]{2,1,0:T(8,128)(2,1)} %param.48) | copy-start | bytes 6291460
  7.2 56.1 %copy-start.12 = (u32[32]{0:T(128)S(1)}, u32[32]{0:T(128)}, u32[]{:S(2)}) copy-start(u32[32]{0:T(128)} %constant.128) | copy-start | bytes 388
  7.2 38.1 %copy-start.3 = (s32[3,6]{1,0:T(4,128)S(1)}, s32[3,6]{1,0:T(4,128)}, u32[]{:S(2)}) copy-start(s32[3,6]{1,0:T(4,128)} %param.45) | copy-start | bytes 220
  7.2 38.2 %copy-start.2 = (bf16[2048,64]{0,1:T(8,128)(2,1)S(1)}, bf16[2048,64]{0,1:T(8,128)(2,1)}, u32[]{:S(2)}) copy-start(bf16[2048,64]{0,1:T(8,128)(2,1)} %param.33) | copy-start | bytes 786436
  7.2 38.2 %copy-start.9 = (f32[64]{0:T(128)S(1)}, f32[64]{0:T(128)}, u32[]{:S(2)}) copy-start(f32[64]{0:T(128)} %param.34) | copy-start | bytes 772
  7.2 38.2 %copy-start.8 = (f32[3,64]{1,0:T(4,128)S(1)}, f32[3,64]{1,0:T(4,128)}, u32[]{:S(2)}) copy-start(f32[3,64]{1,0:T(4,128)} %param.36) | copy-start | bytes 2308
  7.2 55.0 %copy-start.4 = (bf16[4,6144]{1,0:T(4,128)(2,1)S(1)}, bf16[4,6144]{1,0:T(4,128)(2,1)}, u32[]{:S(2)}) copy-start(bf16[4,6144]{1,0:T(4,128)(2,1)} %param.38) | copy-start | bytes 147460
  7.2 55.8 %copy-start.10 = (f32[64]{0:T(128)S(1)}, f32[64]{0:T(128)}, u32[]{:S(2)}) copy-start(f32[64]{0:T(128)} %param.37) | copy-start | bytes 772
  7.3 55.9 %copy-start.7 = (f32[2048]{0:T(1024)S(1)}, f32[2048]{0:T(1024)}, u32[]{:S(2)}) copy-start(f32[2048]{0:T(1024)} %param.43) | copy-start | bytes 24580
  7.3 65.2 %copy-start.1 = (bf16[3,3,6144]{2,1,0:T(4,128)(2,1)S(1)}, bf16[3,3,6144]{2,1,0:T(4,128)(2,1)}, u32[]{:S(2)}) copy-start(bf16[3,3,6144]{2,1,0:T(4,128)(2,1)} %param.27) | copy-start | bytes 331780
  7.3 66.4 %copy-start.5 = (f32[6144]{0:T(1024)S(1)}, f32[6144]{0:T(1024)}, u32[]{:S(2)}) copy-start(f32[6144]{0:T(1024)} %param.39) | copy-start | bytes 73732
  34.4 11.9 %all-to-all-start.1 = ((bf16[16,3,64]{2,1,0:T(4,128)(2,1)}), bf16[16,3,64]{2,1,0:T(4,128)(2,1)S(1)}, u32[]{:S(2)}, u32[]{:S(2)}) async-start(bf16[16,3,64]{2,1,0:T(4,128)(2,1)} %all_to_all.72), calls=%async_computation.1 | async-start | bytes 32768 | tf_op jit(solution)/shard_map/all_to_all | solution.py:75
  44.4 52.0 %copy-start.6 = (f32[4096]{0:T(1024)S(1)}, f32[4096]{0:T(1024)}, u32[]{:S(2)}) copy-start(f32[4096]{0:T(1024)} %param.41) | copy-start | bytes 49156
  46.3 12.5 %all-to-all-start.2 = ((bf16[16,3,64]{2,1,0:T(4,128)(2,1)}), bf16[16,3,64]{2,1,0:T(4,128)(2,1)S(1)}, u32[]{:S(2)}, u32[]{:S(2)}) async-start(bf16[16,3,64]{2,1,0:T(4,128)(2,1)} %all_to_all.76), calls=%async_computation.2 | async-start | bytes 32768 | tf_op jit(solution)/shard_map/all_to_all | solution.py:76
  58.7 10.1 %all-to-all-start = ((bf16[16,3,256]{2,1,0:T(4,128)(2,1)}), bf16[16,3,256]{2,1,0:T(4,128)(2,1)S(1)}, u32[]{:S(2)}, u32[]{:S(2)}) async-start(bf16[16,3,256]{2,1,0:T(4,128)(2,1)} %all_to_all.68), calls=%async_computation | async-start | bytes 65536 | tf_op jit(solution)/shard_map/all_to_all | solution.py:74
  68.9 10.1 %all-to-all-start.3 = ((bf16[16,3,256]{2,1,0:T(4,128)(2,1)}), bf16[16,3,256]{2,1,0:T(4,128)(2,1)S(1)}, u32[]{:S(2)}, u32[]{:S(2)}) async-start(bf16[16,3,256]{2,1,0:T(4,128)(2,1)} %all_to_all.80), calls=%async_computation.3 | async-start | bytes 65536 | tf_op jit(solution)/shard_map/all_to_all | solution.py:73
  72.4 136.1 %all-reduce.3.cloned.1.call-start = ((), (), s32[]{:S(2)}) async-start(), calls=%async_computation.7 | async-start | bytes 196608
  120.8 11.5 %all-to-all-start.4 = ((bf16[16,3,128]{2,1,0:T(4,128)(2,1)}), bf16[16,3,128]{2,1,0:T(4,128)(2,1)S(1)}, u32[]{:S(2)}, u32[]{:S(2)}) async-start(bf16[16,3,128]{2,1,0:T(4,128)(2,1)} %all_to_all.82), calls=%async_computation.4 | async-start | bytes 32768 | tf_op jit(solution)/shard_map/all_to_all | solution.py:129
  125.3 14.1 %copy-start.11 = (bf16[2048,16]{0,1:T(8,128)(2,1)S(1)}, bf16[2048,16]{0,1:T(8,128)(2,1)}, u32[]{:S(2)}) copy-start(bf16[2048,16]{0,1:T(8,128)(2,1)} %param.44) | copy-start | bytes 196612
  133.4 13.9 %all-to-all-start.5 = ((bf16[16,1,2,2048]{3,2,1,0:T(2,128)(2,1)}), bf16[16,1,2,2048]{3,2,1,0:T(2,128)(2,1)S(1)}, u32[]{:S(2)}, u32[]{:S(2)}) async-start(bf16[16,1,2,2048]{3,2,1,0:T(2,128)(2,1)} %bitcast.18), calls=%async_computation.5 | async-start | bytes 262144 | tf_op jit(solution)/shard_map/all_to_all | solution.py:149
  152.7 56.5 %all-to-all-start.6 = ((bf16[16,1,2,2048]{3,2,1,0:T(2,128)(2,1)}), bf16[16,1,2,2048]{3,2,1,0:T(2,128)(2,1)S(1)}, u32[]{:S(2)}, u32[]{:S(2)}) async-start(bf16[16,1,2,2048]{3,2,1,0:T(2,128)(2,1)} %bitcast.22), calls=%async_computation.6 | async-start | bytes 262144 | tf_op jit(solution)/shard_map/all_to_all | solution.py:153
Sparse Core Ops, SparseCore 0:
  120.9 87.4 all-reduce.2
where the time goes:
time: 221 us; the launch traced here: 220 us
  waiting for transfers between devices  73 us (33%)
  blocking collectives  43.3 us (20%)
  matrix products  33.5 us (15%)
  starting transfers between devices  29.5 us (13%)
  between operations  15.2 us (7%)
  other arithmetic  14.1 us (6%)
  local copies, waits for them, and re-layouts  11 us (5%)
    unnamed x2, waiting for transfers between devices  52.2 us
    all_gather x1, blocking collectives, shards(): gathered = lax.all_gather(hidden, 'ep', axis=0, tiled=True)  24.2 us
    all_gather x1, blocking collectives, shards(): lax.all_gather(gated_out, 'ep', axis=0, tiled=True)  19 us
    dot_general x13, matrix products, matmul(): return jnp.dot(left, right, preferred_element_type=jnp.float32)  16.8 us
    dot_general x1, matrix products, shards(): jnp.einsum('sgepn,sgn->sgep', next_state, read_vec, precision=lax.Precisi...  16.8 us
    add x1, other arithmetic, shards(): decay_rate[..., None, None] * carried  6.99 us
    all_to_all x1, waiting for transfers between devices, shards(): lax.all_to_all(outbound, 'ep', split_axis=0, concat_axis=0, tiled=True)  6.66 us
    all_to_all x1, starting transfers between devices, shards(): lax.all_to_all(read_part, 'ep', split_axis=0, concat_axis=1, tiled=True)  5.97 us
  transfers between devices with their start and end apart: 8, of which 5 were waited for; matrix products, arithmetic and copies ran while one was open for 13% of the time, Pallas kernels for 0%

commit v1 on v0

--- a/solution.py
+++ b/solution.py
@@ -9,6 +9,18 @@
 CAP = 2
 epsilon = 1e-06
 routed_scale = 2.5
+
+
+def _draft_widths(original, named_axis, out_dim, which_dim):
+    return jnp.concatenate(
+        lax.all_to_all(
+            jnp.stack(jnp.split(original, lax.psum(1, axis_name=named_axis), axis=out_dim)),
+            split_axis=0,
+            concat_axis=0,
+            axis_name=named_axis,
+        ),
+        axis=which_dim,
+    )
 
 
 def row_scale(values):
@@ -73,7 +85,7 @@
         lax.all_to_all(gate_part, "ep", split_axis=0, concat_axis=1, tiled=True),
         lax.all_to_all(input_part, "ep", split_axis=0, concat_axis=1, tiled=True),
         lax.all_to_all(write_part, "ep", split_axis=0, concat_axis=1, tiled=True),
-        lax.all_to_all(read_part, "ep", split_axis=0, concat_axis=1, tiled=True),
+        _draft_widths(read_part, named_axis="ep", out_dim=0, which_dim=1),
     )
     normed_local = lax.dynamic_slice_in_dim(normed, device_index * local_rows, local_rows, 0)
     step_raw = matmul(normed_local, step_proj)

time: 221 us -> 237 us (1.072)
  local copies, waits for them, and re-layouts: 11 us -> 19.4 us
  waiting for transfers between devices: 73 us -> 80.8 us
    unnamed x33 -> x48, local copies, waits for them, and re-layouts: 1.12 us -> 9.61 us
    unnamed x2, waiting for transfers between devices: 52.2 us -> 59.8 us
    all_to_all x1, waiting for transfers between devices: 0.01 us -> 5.78 us  [shards(): lax.all_to_all(write_part, 'ep', split_axis=0, concat_axis=1, tiled=True)]
    all_to_all x1, waiting for transfers between devices: 5.78 us -> 0.01 us  [_draft_widths(): lax.all_to_all(jnp.stack(jnp.split(original, lax.psum(1, axis_name=named_...]
    all_to_all x1, starting transfers between devices: 5.97 us -> 3.49 us  [_draft_widths(): lax.all_to_all(jnp.stack(jnp.split(original, lax.psum(1, axis_name=named_...]
    all_to_all x1, starting transfers between devices: 3.49 us -> 5.97 us  [shards(): lax.all_to_all(write_part, 'ep', split_axis=0, concat_axis=1, tiled=True)]
where the time goes in v1:
time: 237 us; the launch traced here: 236 us
  waiting for transfers between devices  80.8 us (34%)
  blocking collectives  43.3 us (18%)
  matrix products  33.6 us (14%)
  starting transfers between devices  29.5 us (12%)
  local copies, waits for them, and re-layouts  19.4 us (8%)
  between operations  15.2 us (6%)
  other arithmetic  14.1 us (6%)
    unnamed x2, waiting for transfers between devices  59.8 us
    all_gather x1, blocking collectives, shards(): gathered = lax.all_gather(hidden, 'ep', axis=0, tiled=True)  24.2 us
    all_gather x1, blocking collectives, shards(): lax.all_gather(gated_out, 'ep', axis=0, tiled=True)  19 us
    dot_general x13, matrix products, matmul(): return jnp.dot(left, right, preferred_element_type=jnp.float32)  16.8 us
    dot_general x1, matrix products, shards(): jnp.einsum('sgepn,sgn->sgep', next_state, read_vec, precision=lax.Precisi...  16.8 us
    unnamed x48, local copies, waits for them, and re-layouts  9.61 us
    add x1, other arithmetic, shards(): decay_rate[..., None, None] * carried  6.99 us
    all_to_all x1, waiting for transfers between devices, shards(): lax.all_to_all(outbound, 'ep', split_axis=0, concat_axis=0, tiled=True)  6.71 us
  transfers between devices with their start and end apart: 8, of which 5 were waited for; matrix products, arithmetic and copies ran while one was open for 13% of the time, Pallas kernels for 0%

profile of v1, /device:TPU:0, one launch (start us, length us, event | category | flops | bytes accessed | tf_op | source)
XLA Modules:
  0.0 235.7 jit_solution(10095147501864933205)
XLA Ops:
  7.3 24.2 %all-gather = bf16[16,3,2048]{2,1,0:T(4,128)(2,1)S(1)} all-gather(bf16[1,3,2048]{2,1,0:T(4,128)(2,1)} %bitcast.170), channel_id=1, replica_groups=mesh['grp'=2,'ep'=16] {'ep'}, dimensions={0}, use_global_device_ids=true | all-gather | bytes 208896 | tf_op jit(solution)/shard_map/all_gather | solution.py:77
  31.8 0.8 multiply_convert_fusion
  32.6 1.2 convolution_convert_fusion.6
  42.8 3.5 %all-to-all-start.2 = ((bf16[16,3,64]{2,1,0:T(4,128)(2,1)}), bf16[16,3,64]{2,1,0:T(4,128)(2,1)S(1)}, u32[]{:S(2)}, u32[]{:S(2)}) async-start(bf16[16,3,64]{2,1,0:T(4,128)(2,1)} %constant_dynamic-update-slice_fusion), calls=%async_computation.2 | async-start | bytes 32768 | tf_op jit(solution)/shard_map/all_to_all | solution.py:16
  47.0 0.8 fusion.42
  47.8 1.5 convolution_convert_fusion.4
  49.3 1.2 convolution_convert_fusion.7
  50.5 1.5 convolution_convert_fusion.5
  52.8 0.8 gather_fusion.1
  54.7 6.0 %all-to-all-start.1 = ((bf16[16,3,64]{2,1,0:T(4,128)(2,1)}), bf16[16,3,64]{2,1,0:T(4,128)(2,1)S(1)}, u32[]{:S(2)}, u32[]{:S(2)}) async-start(bf16[16,3,64]{2,1,0:T(4,128)(2,1)} %all_to_all.61), calls=%async_computation.1 | async-start | bytes 32768 | tf_op jit(solution)/shard_map/all_to_all | solution.py:87
  61.4 5.8 %all-to-all-done.1 = bf16[16,3,64]{2,1,0:T(4,128)(2,1)S(1)} async-done(((bf16[16,3,64]{2,1,0:T(4,128)(2,1)}), bf16[16,3,64]{2,1,0:T(4,128)(2,1)S(1)}, u32[]{:S(2)}, u32[]{:S(2)}) %all-to-all-start.1) | async-done | bytes 6176 | tf_op jit(solution)/shard_map/all_to_all | solution.py:87
  67.2 3.5 %all-to-all-start = ((bf16[16,3,256]{2,1,0:T(4,128)(2,1)}), bf16[16,3,256]{2,1,0:T(4,128)(2,1)S(1)}, u32[]{:S(2)}, u32[]{:S(2)}) async-start(bf16[16,3,256]{2,1,0:T(4,128)(2,1)} %all_to_all.57), calls=%async_computation | async-start | bytes 65536 | tf_op jit(solution)/shard_map/all_to_all | solution.py:86
  73.1 4.2 %all-to-all-done = bf16[16,3,256]{2,1,0:T(4,128)(2,1)S(1)} async-done(((bf16[16,3,256]{2,1,0:T(4,128)(2,1)}), bf16[16,3,256]{2,1,0:T(4,128)(2,1)S(1)}, u32[]{:S(2)}, u32[]{:S(2)}) %all-to-all-start) | async-done | bytes 24608 | tf_op jit(solution)/shard_map/all_to_all | solution.py:86
  77.3 3.5 %all-to-all-start.3 = ((bf16[16,3,256]{2,1,0:T(4,128)(2,1)}), bf16[16,3,256]{2,1,0:T(4,128)(2,1)S(1)}, u32[]{:S(2)}, u32[]{:S(2)}) async-start(bf16[16,3,256]{2,1,0:T(4,128)(2,1)} %all_to_all.66), calls=%async_computation.3 | async-start | bytes 65536 | tf_op jit(solution)/shard_map/all_to_all | solution.py:85
  80.9 0.9 fusion.25
  83.1 4.3 %all-to-all-done.3 = bf16[16,3,256]{2,1,0:T(4,128)(2,1)S(1)} async-done(((bf16[16,3,256]{2,1,0:T(4,128)(2,1)}), bf16[16,3,256]{2,1,0:T(4,128)(2,1)S(1)}, u32[]{:S(2)}, u32[]{:S(2)}) %all-to-all-start.3) | async-done | bytes 24608 | tf_op jit(solution)/shard_map/all_to_all | solution.py:85
  87.6 16.8 %fusion = f32[3,8,1,8,64]{4,2,3,1,0:T(1,128)S(1)} fusion(f32[3,8,128,1,1]{2,3,4,1,0:T(1,128)S(1)} %bitcast.169, f32[3,8,8,64,128]{4,3,2,1,0:T(8,128)} %bitcast.160, f32[3,8,128]{2,1,0:T(8,128)S(1)} %bitcast.166, f32[3,8,8,64]{3,2,1,0:T(8,128)S(1)} %broadcast_multiply_fusion.1, f32[3,8,8]{2,1,0:T(8,128)S(1)} %mul.238), kind=kOutput, calls=%fused_computation.4 | convolution fusion | flops 23592960 | bytes 6415104 | tf_op jit(solution)/shard_map/sgepn,sgn->sgep/dot_general | solution.py:117
  104.9 19.0 %all-gather.1 = bf16[16,3,4096]{2,1,0:T(4,128)(2,1)S(1)} all-gather(bf16[1,3,4096]{2,1,0:T(4,128)(2,1)S(1)} %fusion.40), channel_id=1, replica_groups=mesh['grp'=2,'ep'=16] {'ep'}, dimensions={0}, use_global_device_ids=true | all-gather | bytes 417792 | tf_op jit(solution)/shard_map/all_gather | solution.py:128
  124.3 1.5 fusion.21
  126.5 3.5 %all-to-all-start.4 = ((bf16[16,3,128]{2,1,0:T(4,128)(2,1)}), bf16[16,3,128]{2,1,0:T(4,128)(2,1)S(1)}, u32[]{:S(2)}, u32[]{:S(2)}) async-start(bf16[16,3,128]{2,1,0:T(4,128)(2,1)} %all_to_all.68), calls=%async_computation.4 | async-start | bytes 32768 | tf_op jit(solution)/shard_map/all_to_all | solution.py:141
  130.0 1.0 convolution_convert_fusion.2
  131.1 1.0 convolution_convert_fusion.3
  132.8 1.0 broadcast_multiply_fusion
  133.8 7.0 %multiply_add_fusion = f32[3,64,64,128]{3,2,1,0:T(8,128)} fusion(f32[3,64,64,128]{3,2,1,0:T(8,128)} %param.28, f32[3,64,128]{2,1,0:T(8,128)S(1)} %broadcast_bitcast_fusion, f32[3,64,64]{2,1,0:T(8,128)S(1)} %broadcast_multiply_fusion, f32[3,64]{1,0:T(4,128)S(1)} %get-tuple-element.11), kind=kLoop, calls=%fused_computation.3 | loop fusion | flops 4718592 | bytes 12731136 | tf_op jit(solution)/shard_map/add | solution.py:114
  141.9 6.0 %all-to-all-start.5 = ((bf16[16,1,2,2048]{3,2,1,0:T(2,128)(2,1)}), bf16[16,1,2,2048]{3,2,1,0:T(2,128)(2,1)S(1)}, u32[]{:S(2)}, u32[]{:S(2)}) async-start(bf16[16,1,2,2048]{3,2,1,0:T(2,128)(2,1)} %bitcast.34), calls=%async_computation.5 | async-start | bytes 262144 | tf_op jit(solution)/shard_map/all_to_all | solution.py:161
  148.1 0.9 gather_fusion.2
  149.2 6.7 %all-to-all-done.5 = bf16[16,1,2,2048]{3,2,1,0:T(2,128)(2,1)S(1)} async-done(((bf16[16,1,2,2048]{3,2,1,0:T(2,128)(2,1)}), bf16[16,1,2,2048]{3,2,1,0:T(2,128)(2,1)S(1)}, u32[]{:S(2)}, u32[]{:S(2)}) %all-to-all-start.5) | async-done | bytes 131104 | tf_op jit(solution)/shard_map/all_to_all | solution.py:161
  155.9 2.1 fusion.11
  158.0 2.5 %convolution_convert_fusion = bf16[32,2048]{1,0:T(8,128)(2,1)S(1)} fusion(bf16[1,512,2048]{2,1,0:T(8,128)(2,1)S(1)} %copy-done, bf16[32,2048]{1,0:T(8,128)(2,1)S(1)} %reshape_squeeze.3, bf16[1,2048,512]{2,1,0:T(8,128)(2,1)} %param.47, f32[32,512]{1,0:T(8,128)S(1)} %fusion.11), kind=kOutput, calls=%fused_computation.11 | convolution fusion | flops 134381568 | bytes 4521984 | tf_op jit(solution)/shard_map/dot_general | solution.py:31
  161.3 3.5 %all-to-all-start.6 = ((bf16[16,1,2,2048]{3,2,1,0:T(2,128)(2,1)}), bf16[16,1,2,2048]{3,2,1,0:T(2,128)(2,1)S(1)}, u32[]{:S(2)}, u32[]{:S(2)}) async-start(bf16[16,1,2,2048]{3,2,1,0:T(2,128)(2,1)} %bitcast.38), calls=%async_computation.6 | async-start | bytes 262144 | tf_op jit(solution)/shard_map/all_to_all | solution.py:165
  164.9 59.8 %all-reduce.3.cloned.1.call-done = bf16[48,1024]{1,0:T(8,128)(2,1)} async-done(((bf16[48,1024]{1,0:T(8,128)(2,1)}), bf16[48,1024]{1,0:T(8,128)(2,1)}) %all-reduce.3.cloned.1.call-update) | async-done | bytes 98320
  226.3 2.6 %fusion.7 = bf16[3,2048]{1,0:T(4,128)(2,1)} fusion(bf16[512,2048]{1,0:T(8,128)(2,1)} %param.51, f32[3,2048]{1,0:T(4,128)S(1)} %multiply_reduce_fusion.2, bf16[16,3,128]{2,1,0:T(4,128)(2,1)S(1)} %all-to-all-done.4, f32[3,1024]{1,0:T(4,128)S(1)} %dynamic-slice_convert_fusion, f32[3]{0:T(128)S(1)} %add_rsqrt_fusion.1), kind=kOutput, calls=%fused_computation.14 | convolution fusion | flops 6328320 | bytes 2158604 | tf_op jit(solution)/shard_map/dot_general | solution.py:31
  (115 shorter events, 22.2 us)
Async XLA Ops:
  7.2 150.8 %copy-start = (bf16[1,512,2048]{2,1,0:T(8,128)(2,1)S(1)}, bf16[1,512,2048]{2,1,0:T(8,128)(2,1)}, u32[]{:S(2)}) copy-start(bf16[1,512,2048]{2,1,0:T(8,128)(2,1)} %param.48) | copy-start | bytes 6291460
  7.2 64.5 %copy-start.12 = (u32[32]{0:T(128)S(1)}, u32[32]{0:T(128)}, u32[]{:S(2)}) copy-start(u32[32]{0:T(128)} %constant.128) | copy-start | bytes 388
  7.2 46.6 %copy-start.3 = (s32[3,6]{1,0:T(4,128)S(1)}, s32[3,6]{1,0:T(4,128)}, u32[]{:S(2)}) copy-start(s32[3,6]{1,0:T(4,128)} %param.45) | copy-start | bytes 220
  7.2 46.6 %copy-start.8 = (f32[3,64]{1,0:T(4,128)S(1)}, f32[3,64]{1,0:T(4,128)}, u32[]{:S(2)}) copy-start(f32[3,64]{1,0:T(4,128)} %param.36) | copy-start | bytes 2308
  7.2 46.6 %copy-start.9 = (f32[64]{0:T(128)S(1)}, f32[64]{0:T(128)}, u32[]{:S(2)}) copy-start(f32[64]{0:T(128)} %param.34) | copy-start | bytes 772
  7.2 46.6 %copy-start.2 = (bf16[2048,64]{0,1:T(8,128)(2,1)S(1)}, bf16[2048,64]{0,1:T(8,128)(2,1)}, u32[]{:S(2)}) copy-start(bf16[2048,64]{0,1:T(8,128)(2,1)} %param.33) | copy-start | bytes 786436
  7.2 64.1 %copy-start.4 = (bf16[4,6144]{1,0:T(4,128)(2,1)S(1)}, bf16[4,6144]{1,0:T(4,128)(2,1)}, u32[]{:S(2)}) copy-start(bf16[4,6144]{1,0:T(4,128)(2,1)} %param.38) | copy-start | bytes 147460
  7.2 64.3 %copy-start.10 = (f32[64]{0:T(128)S(1)}, f32[64]{0:T(128)}, u32[]{:S(2)}) copy-start(f32[64]{0:T(128)} %param.37) | copy-start | bytes 772
  7.3 64.3 %copy-start.7 = (f32[2048]{0:T(1024)S(1)}, f32[2048]{0:T(1024)}, u32[]{:S(2)}) copy-start(f32[2048]{0:T(1024)} %param.43) | copy-start | bytes 24580
  7.3 73.6 %copy-start.1 = (bf16[3,3,6144]{2,1,0:T(4,128)(2,1)S(1)}, bf16[3,3,6144]{2,1,0:T(4,128)(2,1)}, u32[]{:S(2)}) copy-start(bf16[3,3,6144]{2,1,0:T(4,128)(2,1)} %param.27) | copy-start | bytes 331780
  7.3 74.8 %copy-start.5 = (f32[6144]{0:T(1024)S(1)}, f32[6144]{0:T(1024)}, u32[]{:S(2)}) copy-start(f32[6144]{0:T(1024)} %param.39) | copy-start | bytes 73732
  42.8 11.9 %all-to-all-start.2 = ((bf16[16,3,64]{2,1,0:T(4,128)(2,1)}), bf16[16,3,64]{2,1,0:T(4,128)(2,1)S(1)}, u32[]{:S(2)}, u32[]{:S(2)}) async-start(bf16[16,3,64]{2,1,0:T(4,128)(2,1)} %constant_dynamic-update-slice_fusion), calls=%async_computation.2 | async-start | bytes 32768 | tf_op jit(solution)/shard_map/all_to_all | solution.py:16
  52.8 52.0 %copy-start.6 = (f32[4096]{0:T(1024)S(1)}, f32[4096]{0:T(1024)}, u32[]{:S(2)}) copy-start(f32[4096]{0:T(1024)} %param.41) | copy-start | bytes 49156
  54.7 12.5 %all-to-all-start.1 = ((bf16[16,3,64]{2,1,0:T(4,128)(2,1)}), bf16[16,3,64]{2,1,0:T(4,128)(2,1)S(1)}, u32[]{:S(2)}, u32[]{:S(2)}) async-start(bf16[16,3,64]{2,1,0:T(4,128)(2,1)} %all_to_all.61), calls=%async_computation.1 | async-start | bytes 32768 | tf_op jit(solution)/shard_map/all_to_all | solution.py:87
  67.2 10.1 %all-to-all-start = ((bf16[16,3,256]{2,1,0:T(4,128)(2,1)}), bf16[16,3,256]{2,1,0:T(4,128)(2,1)S(1)}, u32[]{:S(2)}, u32[]{:S(2)}) async-start(bf16[16,3,256]{2,1,0:T(4,128)(2,1)} %all_to_all.57), calls=%async_computation | async-start | bytes 65536 | tf_op jit(solution)/shard_map/all_to_all | solution.py:86
  77.3 10.1 %all-to-all-start.3 = ((bf16[16,3,256]{2,1,0:T(4,128)(2,1)}), bf16[16,3,256]{2,1,0:T(4,128)(2,1)S(1)}, u32[]{:S(2)}, u32[]{:S(2)}) async-start(bf16[16,3,256]{2,1,0:T(4,128)(2,1)} %all_to_all.66), calls=%async_computation.3 | async-start | bytes 65536 | tf_op jit(solution)/shard_map/all_to_all | solution.py:85
  126.5 14.3 %all-to-all-start.4 = ((bf16[16,3,128]{2,1,0:T(4,128)(2,1)}), bf16[16,3,128]{2,1,0:T(4,128)(2,1)S(1)}, u32[]{:S(2)}, u32[]{:S(2)}) async-start(bf16[16,3,128]{2,1,0:T(4,128)(2,1)} %all_to_all.68), calls=%async_computation.4 | async-start | bytes 32768 | tf_op jit(solution)/shard_map/all_to_all | solution.py:141
  130.0 94.7 %all-reduce.3.cloned.1.call-start = ((), (), s32[]{:S(2)}) async-start(), calls=%async_computation.7 | async-start | bytes 196608
  133.8 14.1 %copy-start.11 = (bf16[2048,16]{0,1:T(8,128)(2,1)S(1)}, bf16[2048,16]{0,1:T(8,128)(2,1)}, u32[]{:S(2)}) copy-start(bf16[2048,16]{0,1:T(8,128)(2,1)} %param.44) | copy-start | bytes 196612
  141.9 14.0 %all-to-all-start.5 = ((bf16[16,1,2,2048]{3,2,1,0:T(2,128)(2,1)}), bf16[16,1,2,2048]{3,2,1,0:T(2,128)(2,1)S(1)}, u32[]{:S(2)}, u32[]{:S(2)}) async-start(bf16[16,1,2,2048]{3,2,1,0:T(2,128)(2,1)} %bitcast.34), calls=%async_computation.5 | async-start | bytes 262144 | tf_op jit(solution)/shard_map/all_to_all | solution.py:161
  161.3 64.1 %all-to-all-start.6 = ((bf16[16,1,2,2048]{3,2,1,0:T(2,128)(2,1)}), bf16[16,1,2,2048]{3,2,1,0:T(2,128)(2,1)S(1)}, u32[]{:S(2)}, u32[]{:S(2)}) async-start(bf16[16,1,2,2048]{3,2,1,0:T(2,128)(2,1)} %bitcast.38), calls=%async_computation.6 | async-start | bytes 262144 | tf_op jit(solution)/shard_map/all_to_all | solution.py:165
Sparse Core Ops, SparseCore 0:
  134.2 90.3 all-reduce.2
